TPU v7x, 32 devices: a whole 2x2x4 slice. The times are simulated.
32 devices in a mesh: ep: 8 (over z, x), tp: 4 (over y, core).
Axes of the slice: x: 2, y: 2, z: 4, core: 2. Of those that a mesh axis runs over, the one named last changes fastest.
Arguments:
- tokens: bfloat16 [32, 2048], P('ep'), may hold values from -6 to 6
- norm_gain: bfloat16 [2048], replicated, may hold values from 0.099609375 to 1.8984375
- in_weight: bfloat16 [2048, 1024], P(None, 'tp'), may hold values from -0.125 to 0.125
- decay_rate: float32 [64, 64], P('tp'), may hold values from 0.05 to 1
- frequency: float32 [64, 64], P('tp'), may hold values from -3 to 3
- log_step: float32 [64], P('tp'), may hold values from -2.3 to 0.7
- input_real: float32 [64, 64, 16], P('tp'), may hold values from -1.75 to 1.75
- input_imag: float32 [64, 64, 16], P('tp'), may hold values from -1.75 to 1.75
- output_real: float32 [64, 16, 64], P('tp'), may hold values from -0.5 to 0.5
- output_imag: float32 [64, 16, 64], P('tp'), may hold values from -0.5 to 0.5
- skip_gain: float32 [1024], P('tp'), may hold values from -3 to 3
- state_real: float32 [32, 64, 64], P('ep', 'tp'), may hold values from -6 to 6
- state_imag: float32 [32, 64, 64], P('ep', 'tp'), may hold values from -6 to 6
- out_weight: bfloat16 [1024, 2048], P('tp'), may hold values from -0.1875 to 0.1875
- ffn_gain: bfloat16 [2048], replicated, may hold values from 0.099609375 to 1.8984375
- expert_ids: int32 [32, 2], replicated, may hold values from 0 to 7, all different within a row; in each aligned block of 4 rows (0 to 3, 4 to 7, ...) at most 2 rows name the same one
- route_weights: float32 [32, 2], P('ep'), may hold values from 0.2 to 1
- gate_weight: bfloat16 [2048, 65536], P(None, ('ep', 'tp')), may hold values from -0.125 to 0.125
- up_weight: bfloat16 [2048, 65536], P(None, ('ep', 'tp')), may hold values from -0.125 to 0.125
- down_weight: bfloat16 [65536, 2048], P('ep', 'tp'), may hold values from -0.0625 to 0.0625
Outputs:
- mixed: bfloat16 [32, 2048], P('ep', 'tp')
- new_real: float32 [32, 64, 64], P('ep', 'tp')
- new_imag: float32 [32, 64, 64], P('ep', 'tp')
Inputs may be any that keep to these rules, and one draw needn't show every extreme that they name: `expert_ids`: the 2 experts of a row differ. In each aligned block of 4 rows (the rows of one index of ep) no expert is named by more than 2 rows, and in some blocks one expert is named by exactly 2 rows.
All inputs are finite; a program needn't handle non-finite values.
Results may differ from a plain program's by a relative error of at most 0.007.
Values may be sent and summed in bfloat16 or wider, within the bound.
A program may use at most 64 MiB of HBM per device.

v0:
```python
import jax
import jax.numpy as jnp
from jax import lax
from jax.sharding import PartitionSpec as P

EXPERTS = 8
EPSILON = 1e-06


def rms_scale(values, gain):
    floats = values.astype(jnp.float32)
    return (
        floats
        * lax.rsqrt(jnp.mean(floats * floats, axis=-1, keepdims=True) + EPSILON)
        * gain.astype(jnp.float32)
    )


def discretize(decay_rate, frequency, log_step, input_real, input_imag):
    step_size = jnp.exp(log_step)[:, None]
    lam_real = -decay_rate
    magnitude = jnp.exp(lam_real * step_size)
    turned = frequency * step_size
    bar_real = magnitude * jnp.cos(turned)
    bar_imag = magnitude * jnp.sin(turned)
    denom = lam_real * lam_real + frequency * frequency
    minus_one = bar_real - 1.0
    factor_real = (minus_one * lam_real + bar_imag * frequency) / denom
    factor_imag = (bar_imag * lam_real - minus_one * frequency) / denom
    b_real = factor_real[..., None] * input_real - factor_imag[..., None] * input_imag
    b_imag = factor_real[..., None] * input_imag + factor_imag[..., None] * input_real
    return (bar_real, bar_imag, b_real, b_imag)


def state_update(
    projected,
    state_real,
    state_imag,
    decay_rate,
    frequency,
    log_step,
    input_real,
    input_imag,
    output_real,
    output_imag,
    skip_gain,
):
    bar_real, bar_imag, b_real, b_imag = discretize(
        decay_rate, frequency, log_step, input_real, input_imag
    )
    count, groups, _ = state_real.shape
    high = lax.Precision.HIGHEST
    grouped = projected.astype(jnp.float32).reshape(count, groups, -1)
    drive_real = jnp.einsum("sgp,gnp->sgn", grouped, b_real, precision=high)
    drive_imag = jnp.einsum("sgp,gnp->sgn", grouped, b_imag, precision=high)
    new_real = bar_real * state_real - bar_imag * state_imag + drive_real
    new_imag = bar_real * state_imag + bar_imag * state_real + drive_imag
    readout = jnp.einsum("sgn,gpn->sgp", new_real, output_real, precision=high) - jnp.einsum(
        "sgn,gpn->sgp", new_imag, output_imag, precision=high
    )
    readout = readout.reshape(count, -1) + skip_gain * grouped.reshape(count, -1)
    return (jax.nn.gelu(readout).astype(jnp.bfloat16), new_real, new_imag)


def slot_table(own_ids, own_weights, slot_count):
    expert_range = jnp.arange(EXPERTS, dtype=jnp.int32)
    onehot = (own_ids[:, :, None] == expert_range).astype(jnp.int32)
    flat = onehot.reshape(-1, EXPERTS)
    before = (jnp.cumsum(flat, axis=0) - flat).reshape(onehot.shape)
    slots = jnp.arange(slot_count, dtype=jnp.int32)
    match = (before[..., None] == slots) & (onehot[..., None] > 0)
    table = jnp.sum(jnp.where(match, own_weights[:, :, None, None], 0.0), axis=1)
    return jnp.transpose(table, (1, 2, 0))


def shards(
    tokens,
    norm_gain,
    in_weight,
    decay_rate,
    frequency,
    log_step,
    input_real,
    input_imag,
    output_real,
    output_imag,
    skip_gain,
    state_real,
    state_imag,
    out_weight,
    ffn_gain,
    expert_ids,
    route_weights,
    gate_weight,
    up_weight,
    down_weight,
):
    normed_in = rms_scale(tokens, norm_gain).astype(jnp.bfloat16)
    projected = jnp.dot(normed_in, in_weight, preferred_element_type=jnp.float32).astype(
        jnp.bfloat16
    )
    activated, new_real, new_imag = state_update(
        projected,
        state_real,
        state_imag,
        decay_rate,
        frequency,
        log_step,
        input_real,
        input_imag,
        output_real,
        output_imag,
        skip_gain,
    )
    delta = lax.psum(jnp.dot(activated, out_weight, preferred_element_type=jnp.float32), "tp")
    hidden_state = (tokens.astype(jnp.float32) + delta).astype(jnp.bfloat16)
    normed = rms_scale(hidden_state, ffn_gain).astype(jnp.bfloat16)
    seq_count, width = normed.shape
    slot_count = seq_count // 2
    group_span = lax.axis_size("ep") // EXPERTS
    my_index = lax.axis_index("ep")
    own_ids = lax.dynamic_slice_in_dim(expert_ids, my_index * seq_count, seq_count, 0)
    unit_weights = jnp.ones(own_ids.shape, jnp.float32)
    select = slot_table(own_ids, unit_weights, slot_count)
    outgoing = jnp.einsum(
        "xcs,sd->xcd", select.astype(jnp.bfloat16), normed, preferred_element_type=jnp.float32
    ).astype(jnp.bfloat16)
    received = lax.all_to_all(
        jnp.repeat(outgoing, group_span, axis=0), "ep", split_axis=0, concat_axis=0, tiled=True
    )
    slot_rows = received.reshape(-1, width)
    gate_pre = jnp.dot(slot_rows, gate_weight, preferred_element_type=jnp.float32)
    up_pre = jnp.dot(slot_rows, up_weight, preferred_element_type=jnp.float32)
    hidden = (jax.nn.silu(gate_pre) * up_pre).astype(jnp.bfloat16)
    quarter = down_weight.shape[1]
    partial_out = jnp.dot(
        lax.all_gather(hidden, "tp", axis=1, tiled=True),
        down_weight,
        preferred_element_type=jnp.float32,
    )
    rounded = partial_out.astype(jnp.bfloat16).reshape(-1, slot_count, quarter)
    returned = lax.all_to_all(rounded, "ep", split_axis=0, concat_axis=0, tiled=True)
    summed = (
        returned.astype(jnp.float32).reshape(EXPERTS, group_span, slot_count, quarter).sum(axis=1)
    )
    weight_table = slot_table(own_ids, route_weights, slot_count)
    routed = jnp.einsum("xcs,xcd->sd", weight_table, summed, precision=lax.Precision.HIGHEST)
    residual = lax.dynamic_slice_in_dim(hidden_state, lax.axis_index("tp") * quarter, quarter, 1)
    mixed = (residual.astype(jnp.float32) + routed).astype(jnp.bfloat16)
    return (mixed, new_real, new_imag)


def solution(mesh):
    in_specs = (
        P("ep", None),
        P(),
        P(None, "tp"),
        P("tp", None),
        P("tp", None),
        P("tp"),
        P("tp", None, None),
        P("tp", None, None),
        P("tp", None, None),
        P("tp", None, None),
        P("tp"),
        P("ep", "tp", None),
        P("ep", "tp", None),
        P("tp", None),
        P(),
        P(),
        P("ep", None),
        P(None, ("ep", "tp")),
        P(None, ("ep", "tp")),
        P("ep", "tp"),
    )
    out_specs = (P("ep", "tp"), P("ep", "tp", None), P("ep", "tp", None))
    return jax.shard_map(shards, mesh=mesh, in_specs=in_specs, out_specs=out_specs, check_vma=False)
```

profile of v0, /device:TPU:0, one launch (start us, length us, event | category | flops | bytes accessed | tf_op | source)
XLA Modules:
  0.0 71.3 jit_solution(13652618909060821899)
XLA Ops:
  0.7 0.8 %constant_dynamic-slice_fusion = s32[4,2]{0,1:T(2,128)S(1)} fusion(s32[32,2]{0,1:T(2,128)} %param.35, s32[]{:T(128)S(6)} %select_n.14), kind=kLoop, calls=%fused_computation.78 | loop fusion | bytes 68 | tf_op jit(solution)/shard_map/dynamic_slice | solution.py:122
  1.5 0.1 copy.71
  1.6 0.1 eq.56
  1.7 0.7 exp.10
  2.4 0.9 %fusion.19 = f32[4]{0:T(128)S(1)} fusion(bf16[4,2048]{1,0:T(4,128)(2,1)} %param.20), kind=kLoop, calls=%fused_computation.32 | loop fusion | flops 24572 | bytes 16400 | tf_op jit(solution)/shard_map/reduce_sum | solution.py:14
  3.3 0.7 convert_element_type.68
  4.0 1.5 %convolution_convert_fusion.2 = bf16[4,256]{1,0:T(4,128)(2,1)S(1)} fusion(bf16[2048,256]{1,0:T(8,128)(2,1)} %param.22, bf16[4,2048]{1,0:T(4,128)(2,1)} %param.20, f32[2048]{0:T(1024)S(1)} %convert_element_type.68, f32[4]{0:T(128)S(1)} %add_rsqrt_fusion.1), kind=kOutput, calls=%fused_computation.13 | convolution fusion | flops 4228096 | bytes 1075216 | tf_op jit(solution)/shard_map/dot_general | solution.py:99
  5.5 0.1 reshape.72
  5.6 0.8 %cosine_multiply_fusion = (f32[16,64]{1,0:T(8,128)S(1)}, f32[16,64]{1,0:T(8,128)S(1)}, f32[16,64]{1,0:T(8,128)S(1)}, f32[16,64]{1,0:T(8,128)S(1)}) fusion(f32[16,64]{1,0:T(8,128)} %param.24, f32[16,64]{1,0:T(8,128)} %param.23, f32[16]{0:T(128)S(1)} %exp.10), kind=kLoop, calls=%fused_computation.51 | loop fusion | flops 17408 | bytes 24640 | tf_op jit(solution)/shard_map/mul | solution.py:24
  6.4 1.2 %fusion.2 = f32[4,16,64]{2,0,1:T(4,128)S(1)} fusion(f32[16,64,16]{1,2,0:T(8,128)} %param.26, f32[16,64,16]{1,2,0:T(8,128)} %param.27, f32[16,64]{1,0:T(8,128)S(1)} %get-tuple-element.21, f32[16,64]{1,0:T(8,128)S(1)} %get-tuple-element.20, f32[4,16,64]{2,1,0:T(8,128)} %param.32, f32[4,16,64]{2,1,0:T(8,128)} %param.31, f32[16,64]{1,0:T(8,128)S(1)} %get-tuple-element.22, ...), kind=kOutput, calls=%fused_computation.6 | convolution fusion | flops 851968 | bytes 198656 | tf_op jit(solution)/shard_map/sgp,gnp->sgn/dot_general | solution.py:55
  7.6 1.2 %fusion.3 = f32[4,16,64]{2,0,1:T(4,128)S(1)} fusion(f32[16,64,16]{1,2,0:T(8,128)} %param.27, f32[16,64,16]{1,2,0:T(8,128)} %param.26, f32[16,64]{1,0:T(8,128)S(1)} %get-tuple-element.21, f32[16,64]{1,0:T(8,128)S(1)} %get-tuple-element.20, f32[4,16,64]{2,1,0:T(8,128)} %param.32, f32[4,16,64]{2,1,0:T(8,128)} %param.31, f32[16,64]{1,0:T(8,128)S(1)} %get-tuple-element.22, ...), kind=kOutput, calls=%fused_computation.8 | convolution fusion | flops 851968 | bytes 198656 | tf_op jit(solution)/shard_map/sgp,gnp->sgn/dot_general | solution.py:54
  8.9 0.1 fusion.43
  9.0 0.7 convert_element_type.80
  9.7 1.2 %fusion.60 = f32[16,4,16]{2,1,0:T(4,128)S(1)} fusion(f32[4,16,64]{2,0,1:T(4,128)S(1)} %fusion.3, f32[16,16,64]{2,1,0:T(8,128)} %param.28), kind=kOutput, calls=%fused_computation.84 | convolution fusion | flops 786432 | bytes 86016 | tf_op jit(solution)/shard_map/sgn,gpn->sgp/dot_general | solution.py:58
  10.9 1.2 %fusion.1 = f32[4,16,16]{2,0,1:T(4,128)S(1)} fusion(f32[16,4,16]{2,1,0:T(4,128)S(1)} %fusion.60, f32[4,16,64]{2,0,1:T(4,128)S(1)} %fusion.2, f32[16,16,64]{2,1,0:T(8,128)} %param.29), kind=kOutput, calls=%fused_computation.4 | convolution fusion | flops 787456 | bytes 90112 | tf_op jit(solution)/shard_map/sgn,gpn->sgp/dot_general | solution.py:58
  12.1 0.1 reshape.73
  12.2 0.9 %fusion.46 = f32[4,2048]{1,0:T(4,128)S(1)} fusion(bf16[256,2048]{1,0:T(8,128)(2,1)S(1)} %copy-done, f32[4,256]{1,0:T(4,128)S(1)} %reshape.73, bf16[4,256]{1,0:T(4,128)(2,1)S(1)} %convolution_convert_fusion.2, f32[256]{0:T(256)} %param.30), kind=kOutput, calls=%fused_computation.69 | convolution fusion | flops 4206592 | bytes 1088512 | tf_op jit(solution)/shard_map/dot_general | solution.py:115
  13.2 12.9 %psum.7 = f32[4,2048]{1,0:T(4,128)S(1)} all-reduce(f32[4,2048]{1,0:T(4,128)S(1)} %fusion.46), channel_id=1, replica_groups=mesh['ep'=8,'tp'=4] {'tp'}, use_global_device_ids=true, to_apply=%region_1.0 | all-reduce | flops 8192 | bytes 65536 | tf_op jit(solution)/shard_map/psum | solution.py:115
  26.1 0.9 %fusion.16 = (f32[4]{0:T(128)S(1)}, bf16[4,2048]{1,0:T(4,128)(2,1)S(1)}) fusion(f32[4,2048]{1,0:T(4,128)S(1)} %psum.7, bf16[4,2048]{1,0:T(4,128)(2,1)} %param.20), kind=kLoop, calls=%fused_computation.29 | loop fusion | flops 49148 | bytes 65552 | tf_op jit(solution)/shard_map/reduce_sum | solution.py:14
  26.9 0.8 %select_reduce_fusion.1 = (f32[4,8,2]{1,0,2:T(4,128)S(1)}, bf16[4,8,2]{1,0,2:T(4,128)(2,1)S(1)}) fusion(f32[4,2]{0,1:T(2,128)} %param.36, s32[4,2,8]{2,0,1:T(4,128)S(1)} %copy.73, pred[4,2,8]{2,0,1:T(4,128)(4,1)S(1)} %copy.74), kind=kLoop, calls=%fused_computation.45 | loop fusion | flops 640 | bytes 736 | tf_op jit(solution)/shard_map/reduce_sum | solution.py:72
  27.7 0.2 convolution_convert_fusion
  28.0 12.5 %all_to_all.10 = bf16[8,2,2048]{2,1,0:T(2,128)(2,1)S(1)} all-to-all(bf16[8,2,2048]{2,1,0:T(2,128)(2,1)S(1)} %copy.75), channel_id=1, replica_groups=mesh['ep'=8,'tp'=4] {'ep'}, dimensions={0} | all-to-all | bytes 131072 | tf_op jit(solution)/shard_map/all_to_all | solution.py:128
  40.5 4.6 %fusion.61 = f32[16,2048]{1,0:T(8,128)S(1)} fusion(bf16[16,2048]{1,0:T(8,128)(2,1)S(1)} %reshape.74, bf16[2048,2048]{1,0:T(8,128)(2,1)} %param.37), kind=kOutput, calls=%fused_computation.85 | convolution fusion | flops 134217728 | bytes 8585216 | tf_op jit(solution)/shard_map/dot_general | solution.py:132
  45.1 4.6 %fusion = bf16[16,2048]{1,0:T(8,128)(2,1)S(1)} fusion(bf16[16,2048]{1,0:T(8,128)(2,1)S(1)} %reshape.74, bf16[2048,2048]{1,0:T(8,128)(2,1)} %param.38, f32[16,2048]{1,0:T(8,128)S(1)} %fusion.61), kind=kOutput, calls=%fused_computation.2 | convolution fusion | flops 134414336 | bytes 8650752 | tf_op jit(solution)/shard_map/dot_general | solution.py:133
  49.7 5.8 %all_gather.3 = bf16[16,8192]{1,0:T(8,128)(2,1)S(1)} all-gather(bf16[16,2048]{1,0:T(8,128)(2,1)S(1)} %fusion), channel_id=1, replica_groups=mesh['ep'=8,'tp'=4] {'tp'}, dimensions={1}, use_global_device_ids=true | all-gather | bytes 327680 | tf_op jit(solution)/shard_map/all_gather | solution.py:137
  55.5 4.6 %convolution_convert_fusion.1 = bf16[16,512]{1,0:T(8,128)(2,1)S(1)} fusion(bf16[16,8192]{1,0:T(8,128)(2,1)S(1)} %all_gather.3, bf16[8192,512]{1,0:T(8,128)(2,1)} %param.39), kind=kOutput, calls=%fused_computation.9 | convolution fusion | flops 134225920 | bytes 8667136 | tf_op jit(solution)/shard_map/dot_general | solution.py:136
  60.0 0.6 reshape.75
  60.7 3.3 %all-to-all-start.1 = ((bf16[8,2,512]{2,1,0:T(2,128)(2,1)}), bf16[8,2,512]{2,1,0:T(2,128)(2,1)S(1)}, u32[]{:S(2)}, u32[]{:S(2)}) async-start(bf16[8,2,512]{2,1,0:T(2,128)(2,1)} %reshape.75), calls=%async_computation.1 | async-start | bytes 32768 | tf_op jit(solution)/shard_map/all_to_all | solution.py:142
  64.0 0.6 copy.77
  64.6 0.6 copy.78
  65.2 5.3 %all-to-all-done.1 = bf16[8,2,512]{2,1,0:T(2,128)(2,1)S(1)} async-done(((bf16[8,2,512]{2,1,0:T(2,128)(2,1)}), bf16[8,2,512]{2,1,0:T(2,128)(2,1)S(1)}, u32[]{:S(2)}, u32[]{:S(2)}) %all-to-all-start.1) | async-done | bytes 16416 | tf_op jit(solution)/shard_map/all_to_all | solution.py:142
  70.5 0.8 %fusion.5 = bf16[4,512]{1,0:T(4,128)(2,1)} fusion(bf16[8,2,512]{2,1,0:T(2,128)(2,1)S(1)} %all-to-all-done.1, f32[4,8,2]{1,0,2:T(4,128)S(1)} %get-tuple-element.15, bf16[4,2048]{1,0:T(4,128)(2,1)S(1)} %get-tuple-element.18, s32[]{:T(128)S(6)} %select_n.13), kind=kOutput, calls=%fused_computation.12 | convolution fusion | flops 399360 | bytes 24836 | tf_op jit(solution)/shard_map/xcs,xcd->sd/dot_general | solution.py:147
  (12 shorter events, 0.3 us)
Async XLA Ops:
  0.6 11.6 %copy-start = (bf16[256,2048]{1,0:T(8,128)(2,1)S(1)}, bf16[256,2048]{1,0:T(8,128)(2,1)}, u32[]{:S(2)}) copy-start(bf16[256,2048]{1,0:T(8,128)(2,1)} %param.33) | copy-start | bytes 3145732
  60.7 9.9 %all-to-all-start.1 = ((bf16[8,2,512]{2,1,0:T(2,128)(2,1)}), bf16[8,2,512]{2,1,0:T(2,128)(2,1)S(1)}, u32[]{:S(2)}, u32[]{:S(2)}) async-start(bf16[8,2,512]{2,1,0:T(2,128)(2,1)} %reshape.75), calls=%async_computation.1 | async-start | bytes 32768 | tf_op jit(solution)/shard_map/all_to_all | solution.py:142
where the time goes:
time: 72.1 us; the launch traced here: 71.3 us
  blocking collectives  31.2 us (43%)
  matrix products  22 us (31%)
  waiting for transfers between devices  5.28 us (7%)
  other arithmetic  4.97 us (7%)
  local copies, waits for them, and re-layouts  3.84 us (5%)
  starting transfers between devices  3.33 us (5%)
  between operations  0.73 us (1%)
    psum x1, blocking collectives, shards(): lax.psum(jnp.dot(activated, out_weight, preferred_element_type=jnp.float3...  12.9 us
    all_to_all x1, blocking collectives, shards(): lax.all_to_all(jnp.repeat(outgoing, group_span, axis=0), 'ep', split_axis...  12.5 us
    all_gather x1, blocking collectives, shards(): lax.all_gather(hidden, 'tp', axis=1, tiled=True)  5.77 us
    all_to_all x1, waiting for transfers between devices, shards(): lax.all_to_all(rounded, 'ep', split_axis=0, concat_axis=0, tiled=True)  5.28 us
    dot_general x1, matrix products, shards(): up_pre = jnp.dot(slot_rows, up_weight, preferred_element_type=jnp.float32)  4.58 us
    dot_general x1, matrix products, shards(): jnp.dot(slot_rows, gate_weight, preferred_element_type=jnp.float32)  4.58 us
    dot_general x1, matrix products, shards(): jnp.dot(lax.all_gather(hidden, 'tp', axis=1, tiled=True), down_weight, pr...  4.56 us
    all_to_all x1, starting transfers between devices, shards(): lax.all_to_all(rounded, 'ep', split_axis=0, concat_axis=0, tiled=True)  3.33 us
  transfers between devices with their start and end apart: 1, of which 1 were waited for; matrix products, arithmetic and copies ran while one was open for 2% of the time, Pallas kernels for 0%

commit v1 on v0

--- a/solution.py
+++ b/solution.py
@@ -5,6 +5,12 @@
 
 EXPERTS = 8
 EPSILON = 1e-06
+
+
+def gathered_along(x, mesh_axis, d):
+    pieces = lax.all_gather(x, mesh_axis, axis=0, tiled=False)
+    out = jnp.concatenate(pieces, axis=d)
+    return out
 
 
 def rms_scale(values, gain):
@@ -134,9 +140,7 @@
     hidden = (jax.nn.silu(gate_pre) * up_pre).astype(jnp.bfloat16)
     quarter = down_weight.shape[1]
     partial_out = jnp.dot(
-        lax.all_gather(hidden, "tp", axis=1, tiled=True),
-        down_weight,
-        preferred_element_type=jnp.float32,
+        gathered_along(hidden, "tp", 1), down_weight, preferred_element_type=jnp.float32
     )
     rounded = partial_out.astype(jnp.bfloat16).reshape(-1, slot_count, quarter)
     returned = lax.all_to_all(rounded, "ep", split_axis=0, concat_axis=0, tiled=True)

time: 72.1 us -> 67 us (0.929)
  matrix products: 22 us -> 15.4 us
  local copies, waits for them, and re-layouts: 3.84 us -> 5.23 us
    dot_general x1, matrix products: 4.58 us -> 1.2 us  [shards(): up_pre = jnp.dot(slot_rows, up_weight, preferred_element_type=jnp.float32)]
    dot_general x1, matrix products: 4.56 us -> 1.18 us  [shards(): jnp.dot(gathered_along(hidden, 'tp', 1), down_weight, preferred_element_t...]
    unnamed x4 -> x11, local copies, waits for them, and re-layouts: 1.24 us -> 2.43 us
where the time goes in v1:
time: 67 us; the launch traced here: 66.3 us
  blocking collectives  31.3 us (47%)
  matrix products  15.4 us (23%)
  waiting for transfers between devices  5.28 us (8%)
  local copies, waits for them, and re-layouts  5.23 us (8%)
  other arithmetic  4.97 us (7%)
  starting transfers between devices  3.33 us (5%)
  between operations  0.78 us (1%)
    psum x1, blocking collectives, shards(): lax.psum(jnp.dot(activated, out_weight, preferred_element_type=jnp.float3...  12.9 us
    all_to_all x1, blocking collectives, shards(): lax.all_to_all(jnp.repeat(outgoing, group_span, axis=0), 'ep', split_axis...  12.5 us
    all_gather x1, blocking collectives, gathered_along(): pieces = lax.all_gather(x, mesh_axis, axis=0, tiled=False)  5.9 us
    all_to_all x1, waiting for transfers between devices, shards(): lax.all_to_all(rounded, 'ep', split_axis=0, concat_axis=0, tiled=True)  5.28 us
    dot_general x1, matrix products, shards(): jnp.dot(slot_rows, gate_weight, preferred_element_type=jnp.float32)  4.73 us
    all_to_all x1, starting transfers between devices, shards(): lax.all_to_all(rounded, 'ep', split_axis=0, concat_axis=0, tiled=True)  3.33 us
    unnamed x11, local copies, waits for them, and re-layouts  2.43 us
    reduce_sum x2, other arithmetic, rms_scale(): jnp.mean(floats * floats, axis=-1, keepdims=True) + EPSILON  1.7 us
  transfers between devices with their start and end apart: 1, of which 1 were waited for; matrix products, arithmetic and copies ran while one was open for 2% of the time, Pallas kernels for 0%

profile of v1, /device:TPU:0, one launch (start us, length us, event | category | flops | bytes accessed | tf_op | source)
XLA Modules:
  0.0 66.3 jit_solution(18267123518737041214)
XLA Ops:
  0.7 0.8 %constant_dynamic-slice_fusion = s32[4,2]{0,1:T(2,128)S(1)} fusion(s32[32,2]{0,1:T(2,128)} %param.35, s32[]{:T(128)S(6)} %select_n.14), kind=kLoop, calls=%fused_computation.78 | loop fusion | bytes 68 | tf_op jit(solution)/shard_map/dynamic_slice | solution.py:128
  1.5 0.1 copy.73
  1.7 0.7 exp.10
  2.4 0.9 %fusion.19 = f32[4]{0:T(128)S(1)} fusion(bf16[4,2048]{1,0:T(4,128)(2,1)} %param.20), kind=kLoop, calls=%fused_computation.32 | loop fusion | flops 24572 | bytes 16400 | tf_op jit(solution)/shard_map/reduce_sum | solution.py:20
  3.3 0.7 %convert_element_type.68 = f32[2048]{0:T(1024)S(1)} convert(bf16[2048]{0:T(1024)(128)(2,1)} %param.21) | non-fusion elementwise | flops 2048 | bytes 12288 | tf_op jit(solution)/shard_map/convert_element_type | solution.py:21
  4.0 1.5 %convolution_convert_fusion.2 = bf16[4,256]{1,0:T(4,128)(2,1)S(1)} fusion(bf16[2048,256]{1,0:T(8,128)(2,1)} %param.22, bf16[4,2048]{1,0:T(4,128)(2,1)} %param.20, f32[2048]{0:T(1024)S(1)} %convert_element_type.68, f32[4]{0:T(128)S(1)} %add_rsqrt_fusion.1), kind=kOutput, calls=%fused_computation.13 | convolution fusion | flops 4228096 | bytes 1075216 | tf_op jit(solution)/shard_map/dot_general | solution.py:105
  5.5 0.1 reshape.78
  5.6 0.8 %cosine_multiply_fusion = (f32[16,64]{1,0:T(8,128)S(1)}, f32[16,64]{1,0:T(8,128)S(1)}, f32[16,64]{1,0:T(8,128)S(1)}, f32[16,64]{1,0:T(8,128)S(1)}) fusion(f32[16,64]{1,0:T(8,128)} %param.24, f32[16,64]{1,0:T(8,128)} %param.23, f32[16]{0:T(128)S(1)} %exp.10), kind=kLoop, calls=%fused_computation.51 | loop fusion | flops 17408 | bytes 24640 | tf_op jit(solution)/shard_map/mul | solution.py:30
  6.4 1.2 %fusion.2 = f32[4,16,64]{2,0,1:T(4,128)S(1)} fusion(f32[16,64,16]{1,2,0:T(8,128)} %param.26, f32[16,64,16]{1,2,0:T(8,128)} %param.27, f32[16,64]{1,0:T(8,128)S(1)} %get-tuple-element.21, f32[16,64]{1,0:T(8,128)S(1)} %get-tuple-element.20, f32[4,16,64]{2,1,0:T(8,128)} %param.32, f32[4,16,64]{2,1,0:T(8,128)} %param.31, f32[16,64]{1,0:T(8,128)S(1)} %get-tuple-element.22, ...), kind=kOutput, calls=%fused_computation.6 | convolution fusion | flops 851968 | bytes 198656 | tf_op jit(solution)/shard_map/sgp,gnp->sgn/dot_general | solution.py:61
  7.6 1.2 %fusion.3 = f32[4,16,64]{2,0,1:T(4,128)S(1)} fusion(f32[16,64,16]{1,2,0:T(8,128)} %param.27, f32[16,64,16]{1,2,0:T(8,128)} %param.26, f32[16,64]{1,0:T(8,128)S(1)} %get-tuple-element.21, f32[16,64]{1,0:T(8,128)S(1)} %get-tuple-element.20, f32[4,16,64]{2,1,0:T(8,128)} %param.32, f32[4,16,64]{2,1,0:T(8,128)} %param.31, f32[16,64]{1,0:T(8,128)S(1)} %get-tuple-element.22, ...), kind=kOutput, calls=%fused_computation.8 | convolution fusion | flops 851968 | bytes 198656 | tf_op jit(solution)/shard_map/sgp,gnp->sgn/dot_general | solution.py:60
  9.0 0.7 %convert_element_type.80 = f32[2048]{0:T(1024)S(1)} convert(bf16[2048]{0:T(1024)(128)(2,1)} %param.34) | non-fusion elementwise | flops 2048 | bytes 12288 | tf_op jit(solution)/shard_map/convert_element_type | solution.py:21
  9.7 1.2 %fusion.60 = f32[16,4,16]{2,1,0:T(4,128)S(1)} fusion(f32[4,16,64]{2,0,1:T(4,128)S(1)} %fusion.3, f32[16,16,64]{2,1,0:T(8,128)} %param.28), kind=kOutput, calls=%fused_computation.84 | convolution fusion | flops 786432 | bytes 86016 | tf_op jit(solution)/shard_map/sgn,gpn->sgp/dot_general | solution.py:64
  10.9 1.2 %fusion.1 = f32[4,16,16]{2,0,1:T(4,128)S(1)} fusion(f32[16,4,16]{2,1,0:T(4,128)S(1)} %fusion.60, f32[4,16,64]{2,0,1:T(4,128)S(1)} %fusion.2, f32[16,16,64]{2,1,0:T(8,128)} %param.29), kind=kOutput, calls=%fused_computation.4 | convolution fusion | flops 787456 | bytes 90112 | tf_op jit(solution)/shard_map/sgn,gpn->sgp/dot_general | solution.py:64
  12.2 0.9 %fusion.46 = f32[4,2048]{1,0:T(4,128)S(1)} fusion(bf16[256,2048]{1,0:T(8,128)(2,1)S(1)} %copy-done, f32[4,256]{1,0:T(4,128)S(1)} %reshape.79, bf16[4,256]{1,0:T(4,128)(2,1)S(1)} %convolution_convert_fusion.2, f32[256]{0:T(256)} %param.30), kind=kOutput, calls=%fused_computation.69 | convolution fusion | flops 4206592 | bytes 1088512 | tf_op jit(solution)/shard_map/dot_general | solution.py:121
  13.2 12.9 %psum.7 = f32[4,2048]{1,0:T(4,128)S(1)} all-reduce(f32[4,2048]{1,0:T(4,128)S(1)} %fusion.46), channel_id=1, replica_groups=mesh['ep'=8,'tp'=4] {'tp'}, use_global_device_ids=true, to_apply=%region_1.0 | all-reduce | flops 8192 | bytes 65536 | tf_op jit(solution)/shard_map/psum | solution.py:121
  26.1 0.9 %fusion.16 = (f32[4]{0:T(128)S(1)}, bf16[4,2048]{1,0:T(4,128)(2,1)S(1)}) fusion(f32[4,2048]{1,0:T(4,128)S(1)} %psum.7, bf16[4,2048]{1,0:T(4,128)(2,1)} %param.20), kind=kLoop, calls=%fused_computation.29 | loop fusion | flops 49148 | bytes 65552 | tf_op jit(solution)/shard_map/reduce_sum | solution.py:20
  26.9 0.8 %select_reduce_fusion.1 = (f32[4,8,2]{1,0,2:T(4,128)S(1)}, bf16[4,8,2]{1,0,2:T(4,128)(2,1)S(1)}) fusion(f32[4,2]{0,1:T(2,128)} %param.36, s32[4,2,8]{2,0,1:T(4,128)S(1)} %copy.75, pred[4,2,8]{2,0,1:T(4,128)(4,1)S(1)} %copy.76), kind=kLoop, calls=%fused_computation.45 | loop fusion | flops 640 | bytes 736 | tf_op jit(solution)/shard_map/reduce_sum | solution.py:78
  27.7 0.2 convolution_convert_fusion
  28.0 12.5 %all_to_all.10 = bf16[8,2,2048]{2,1,0:T(2,128)(2,1)S(1)} all-to-all(bf16[8,2,2048]{2,1,0:T(2,128)(2,1)S(1)} %copy.77), channel_id=1, replica_groups=mesh['ep'=8,'tp'=4] {'ep'}, dimensions={0} | all-to-all | bytes 131072 | tf_op jit(solution)/shard_map/all_to_all | solution.py:134
  40.6 4.7 %fusion.61 = f32[16,2048]{1,0:T(8,128)S(1)} fusion(bf16[16,2048]{1,0:T(8,128)(2,1)S(1)} %reshape.80, bf16[2048,2048]{1,0:T(8,128)(2,1)} %param.37), kind=kOutput, calls=%fused_computation.85 | convolution fusion | flops 134217728 | bytes 8585216 | tf_op jit(solution)/shard_map/dot_general | solution.py:138
  45.3 1.0 %copy-done.1 = bf16[2048,2048]{1,0:T(8,128)(2,1)S(1)} copy-done((bf16[2048,2048]{1,0:T(8,128)(2,1)S(1)}, bf16[2048,2048]{1,0:T(8,128)(2,1)}, u32[]{:S(2)}) %copy-start.1) | copy-done | bytes 8388632
  46.3 1.2 %fusion = bf16[16,2048]{1,0:T(8,128)(2,1)S(1)} fusion(bf16[16,2048]{1,0:T(8,128)(2,1)S(1)} %reshape.80, bf16[2048,2048]{1,0:T(8,128)(2,1)S(1)} %copy-done.1, f32[16,2048]{1,0:T(8,128)S(1)} %fusion.61), kind=kOutput, calls=%fused_computation.2 | convolution fusion | flops 134414336 | bytes 8650752 | tf_op jit(solution)/shard_map/dot_general | solution.py:139
  47.5 5.9 %all-gather = bf16[64,2048]{1,0:T(8,128)(2,1)S(1)} all-gather(bf16[16,2048]{1,0:T(8,128)(2,1)S(1)} %fusion), channel_id=2, replica_groups=mesh['ep'=8,'tp'=4] {'tp'}, dimensions={0}, use_global_device_ids=true | all-gather | bytes 327680 | tf_op jit(solution)/shard_map/all_gather | solution.py:11
  53.4 0.2 copy.78
  53.6 0.2 copy.82
  53.8 1.2 %convolution_convert_fusion.1 = bf16[16,512]{1,0:T(8,128)(2,1)S(1)} fusion(bf16[16,8192]{1,0:T(8,128)(2,1)S(1)} %bitcast.44, bf16[8192,512]{1,0:T(8,128)(2,1)S(1)} %bitcast.43), kind=kOutput, calls=%fused_computation.9 | convolution fusion | flops 134225920 | bytes 8667136 | tf_op jit(solution)/shard_map/dot_general | solution.py:142
  55.0 0.6 reshape.83
  55.6 3.3 %all-to-all-start.1 = ((bf16[8,2,512]{2,1,0:T(2,128)(2,1)}), bf16[8,2,512]{2,1,0:T(2,128)(2,1)S(1)}, u32[]{:S(2)}, u32[]{:S(2)}) async-start(bf16[8,2,512]{2,1,0:T(2,128)(2,1)} %reshape.83), calls=%async_computation.1 | async-start | bytes 32768 | tf_op jit(solution)/shard_map/all_to_all | solution.py:146
  59.0 0.6 copy.80
  59.6 0.6 copy.81
  60.2 5.3 %all-to-all-done.1 = bf16[8,2,512]{2,1,0:T(2,128)(2,1)S(1)} async-done(((bf16[8,2,512]{2,1,0:T(2,128)(2,1)}), bf16[8,2,512]{2,1,0:T(2,128)(2,1)S(1)}, u32[]{:S(2)}, u32[]{:S(2)}) %all-to-all-start.1) | async-done | bytes 16416 | tf_op jit(solution)/shard_map/all_to_all | solution.py:146
  65.5 0.8 %fusion.5 = bf16[4,512]{1,0:T(4,128)(2,1)} fusion(bf16[8,2,512]{2,1,0:T(2,128)(2,1)S(1)} %all-to-all-done.1, f32[4,8,2]{1,0,2:T(4,128)S(1)} %get-tuple-element.15, bf16[4,2048]{1,0:T(4,128)(2,1)S(1)} %get-tuple-element.18, s32[]{:T(128)S(6)} %select_n.13), kind=kOutput, calls=%fused_computation.12 | convolution fusion | flops 399360 | bytes 24836 | tf_op jit(solution)/shard_map/xcs,xcd->sd/dot_general | solution.py:151
  (21 shorter events, 0.6 us)
Async XLA Ops:
  0.6 11.6 %copy-start = (bf16[256,2048]{1,0:T(8,128)(2,1)S(1)}, bf16[256,2048]{1,0:T(8,128)(2,1)}, u32[]{:S(2)}) copy-start(bf16[256,2048]{1,0:T(8,128)(2,1)} %param.33) | copy-start | bytes 3145732
  40.5 5.8 %copy-start.1 = (bf16[2048,2048]{1,0:T(8,128)(2,1)S(1)}, bf16[2048,2048]{1,0:T(8,128)(2,1)}, u32[]{:S(2)}) copy-start(bf16[2048,2048]{1,0:T(8,128)(2,1)} %param.38) | copy-start | bytes 25165828
  40.6 13.2 %slice-start = ((s8[8388608]{0:T(1024)(128)(4,1)}), s8[4194304]{0:T(1024)(128)(4,1)S(1)}, s32[]{:S(2)}) async-start(s8[8388608]{0:T(1024)(128)(4,1)} %bitcast.42), calls=%async_computation.2 | async-start | bytes 8388608
  46.3 7.5 %slice-start.1 = ((s8[8388608]{0:T(1024)(128)(4,1)}), s8[4194304]{0:T(1024)(128)(4,1)S(1)}, s32[]{:S(2)}) async-start(s8[8388608]{0:T(1024)(128)(4,1)} %bitcast.42), calls=%async_computation.3 | async-start | bytes 8388608
  55.6 9.9 %all-to-all-start.1 = ((bf16[8,2,512]{2,1,0:T(2,128)(2,1)}), bf16[8,2,512]{2,1,0:T(2,128)(2,1)S(1)}, u32[]{:S(2)}, u32[]{:S(2)}) async-start(bf16[8,2,512]{2,1,0:T(2,128)(2,1)} %reshape.83), calls=%async_computation.1 | async-start | bytes 32768 | tf_op jit(solution)/shard_map/all_to_all | solution.py:146
